TPU v7x, 128 devices: a whole 4x4x4 slice. The times are simulated.
128 devices in a mesh: rep: 2 (over z_hi), fs: 32 (over z_lo, y, x), tp: 2 (over core).
Axes of the slice: x: 4, y: 4, z: 4 (z_hi: 2, z_lo: 2; z = z_hi * 2 + z_lo), core: 2. Of those that a mesh axis runs over, the one named last changes fastest.
Arguments:
- residual: bfloat16 [32768, 2048], P(('rep', 'fs', 'tp')), may hold values from -6 to 6
- mixer_gain: float32 [2048], replicated, may hold values from 0.1 to 1.9
- gating_proj: bfloat16 [2048, 2048], P('fs', 'tp'), may hold values from -0.125 to 0.125
- spatial_proj: bfloat16 [2048, 2048], P('fs', 'tp'), as said below
- spatial_gain: float32 [2048], replicated, may hold values from 0.1 to 1.9
- spatial_bias: float32 [2048], replicated, may hold values from -3 to 3
- spatial_mix: bfloat16 [32, 128, 128], replicated, may hold values from -0.5 to 0.5
- spatial_offset: float32 [32, 128], replicated, may hold values from 0.5 to 1.5
- mixer_out: bfloat16 [2048, 2048], P('tp', 'fs'), may hold values from -0.125 to 0.125
- channel_gain: float32 [2048], replicated, may hold values from 0.1 to 1.9
- gate_proj: bfloat16 [2048, 2816], P('fs', 'tp'), may hold values from -0.125 to 0.125
- up_proj: bfloat16 [2048, 2816], P('fs', 'tp'), may hold values from -0.125 to 0.125
- conv_taps: float32 [3, 2816], replicated, may hold values from -3.5 to 3.5
- down_proj: bfloat16 [2816, 2048], P('tp', 'fs'), may hold values from -0.109375 to 0.109375
Outputs:
- layer_out: bfloat16 [32768, 2048], P(('rep', 'fs', 'tp'))
Inputs may be any that keep to these rules, and one draw needn't show every extreme that they name: `spatial_proj`: entries are bounded in magnitude by 56 / sqrt(2048).
All inputs are finite; a program needn't handle non-finite values.
Results may differ from a plain program's by a relative error of at most 0.015.
Values may be sent and summed in bfloat16 or wider, within the bound.
No kernel may reach another device: no remote copies, remote signals or barrier semaphores. Data moves between devices by JAX's collectives and lax.ppermute only.
A program may use at most 128 MiB of HBM per device.

v0:
```python
import jax
import jax.numpy as jnp
from jax import lax
from jax.sharding import Mesh
from jax.sharding import PartitionSpec as P

HEAD = 64
GROUP = 2048
BLOCK = 128
SEGMENT = 64
KCONV = 3
SEQ_LEN = 256
FS = ("fs_0", "fs_1", "fs_2")
REP_FS_TP = ("rep", "fs_0", "fs_1", "fs_2", "tp")


def in_order(pieces, dim):
    pieces = jnp.moveaxis(pieces, 0, dim)
    lengths = pieces.shape
    return pieces.reshape(*lengths[:dim], lengths[dim] * lengths[dim + 1], *lengths[dim + 2 :])


def copy_for_each(value, axis):
    devices = lax.axis_size(axis)
    return lax.all_to_all(
        jnp.broadcast_to(value[None], (devices, *value.shape)), axis, 0, 0, tiled=True
    )


def gathered_copies(value, axis, dim):
    return in_order(copy_for_each(value, axis), dim)


def side_by_side(arrays, axis, dim, along):
    widths = [a.shape[along] for a in arrays]
    both = jnp.concatenate(arrays, axis=along)
    out = lax.all_gather(both, axis, axis=dim, tiled=True)
    return tuple(jnp.split(out, [sum(widths[:k]) for k in range(1, len(widths))], axis=along))


def of_everyone(value, axis):
    return copy_for_each(value, axis).sum(axis=0)


def in_one(arrays, axis):
    ends = [0]
    for a in arrays:
        ends.append(ends[-1] + a.size)
    running = of_everyone(jnp.concatenate([a.ravel() for a in arrays]), axis)
    return tuple((running[b:e].reshape(a.shape) for a, b, e in zip(arrays, ends, ends[1:])))


def stacked_from(value, axes, order):
    pieces = value[None]
    for k in order:
        pieces = lax.all_gather(pieces, axes[k], axis=0, tiled=True)
    block = [lax.axis_size(axes[k]) for k in reversed(order)]
    pieces = pieces.reshape(*block, *value.shape)
    turned = sorted(range(len(order)), key=lambda place: order[len(order) - 1 - place])
    return pieces.transpose(*turned, *range(len(order), pieces.ndim)).reshape(-1, *value.shape)


def gather_axes(value, axes, order, dim):
    return in_order(stacked_from(value, axes, order), dim)


def cut_along(value, dim, devices):
    before, after = (value.shape[:dim], value.shape[dim + 1 :])
    return jnp.moveaxis(value.reshape(*before, devices, -1, *after), dim, 0)


def sum_at_owner(value, axis, dim):
    pieces = cut_along(value, dim, lax.axis_size(axis))
    arrived = lax.all_to_all(pieces, axis, split_axis=0, concat_axis=0, tiled=True)
    return arrived.astype(jnp.float32).sum(axis=0)


def round_trip(value):
    return lax.optimization_barrier(value.astype(jnp.bfloat16)).astype(jnp.float32)


def rms_normed(value, gain):
    wide = value.astype(jnp.float32)
    scale = lax.rsqrt(jnp.mean(wide * wide, axis=-1, keepdims=True) + 1e-06)
    return (wide * scale * gain).astype(jnp.bfloat16)


def fold_pair(normed, pieces):
    first = jnp.dot(normed, pieces[0], preferred_element_type=jnp.float32)
    second = jnp.dot(normed, pieces[1], preferred_element_type=jnp.float32)
    return (first, second)


def on_device(
    residual,
    mixer_gain,
    gating_proj,
    spatial_proj,
    spatial_gain,
    spatial_bias,
    spatial_mix,
    spatial_offset,
    mixer_out,
    channel_gain,
    gate_proj,
    up_proj,
    conv_taps,
    down_proj,
):
    position = lax.axis_index("tp")
    rows = gathered_copies(residual, "tp", 0)
    group_rows = rows.shape[0]
    normed = rms_normed(rows, mixer_gain)
    width = gating_proj.shape[1]
    gating, spatial = fold_pair(normed, side_by_side((gating_proj, spatial_proj), FS, 0, 1))
    act_u = jax.nn.gelu(round_trip(gating))
    act_v = jax.nn.gelu(round_trip(spatial))
    total, squares = in_one((jnp.sum(act_v, axis=-1), jnp.sum(act_v * act_v, axis=-1)), "tp")
    mean = (total / GROUP)[:, None]
    var = (squares / GROUP)[:, None] - mean * mean
    gain_here = lax.dynamic_slice_in_dim(spatial_gain, position * width, width)
    bias_here = lax.dynamic_slice_in_dim(spatial_bias, position * width, width)
    vnorm = ((act_v - mean) * lax.rsqrt(var + 1e-05) * gain_here + bias_here).astype(jnp.bfloat16)
    heads_here = width // HEAD
    mix_here = lax.dynamic_slice_in_dim(spatial_mix, position * heads_here, heads_here, 0)
    offset_here = lax.dynamic_slice_in_dim(spatial_offset, position * heads_here, heads_here, 0)
    place = jnp.arange(BLOCK) // SEGMENT
    allowed = place[None, :] <= place[:, None]
    weights = jnp.where(allowed[None], mix_here, jnp.zeros_like(mix_here))
    blocks = vnorm.reshape(group_rows // BLOCK, BLOCK, heads_here, HEAD)
    mixed = jnp.einsum("hij,njhd->nihd", weights, blocks, preferred_element_type=jnp.float32)
    mixed = mixed + offset_here.T[None, :, :, None]
    gated = (act_u * mixed.reshape(group_rows, width)).astype(jnp.bfloat16)
    out_whole = gather_axes(mixer_out, FS, (0, 1, 2), 1)
    part = gated
    mixer_part = sum_at_owner(
        jnp.dot(part, out_whole, preferred_element_type=jnp.float32).astype(jnp.bfloat16), "tp", 0
    )
    middle = (residual.astype(jnp.float32) + mixer_part).astype(jnp.bfloat16)
    rows2 = gathered_copies(middle, "tp", 0)
    normed2 = rms_normed(rows2, channel_gain)
    units = gate_proj.shape[1]
    gate_whole, up_whole = side_by_side((gate_proj, up_proj), FS, 0, 1)
    gate = jnp.dot(normed2, gate_whole, preferred_element_type=jnp.float32)
    up = jnp.dot(normed2, up_whole, preferred_element_type=jnp.float32)
    gate = round_trip(gate)
    up = round_trip(up)
    taps_here = lax.dynamic_slice_in_dim(conv_taps, position * units, units, 1)
    offset = jnp.arange(group_rows) % SEQ_LEN
    conv = taps_here[KCONV - 1] * gate
    for lag in range(1, KCONV):
        shifted = jnp.concatenate([jnp.zeros((lag, units), jnp.float32), gate[:-lag]], axis=0)
        shifted = jnp.where((offset >= lag)[:, None], shifted, 0.0)
        conv = conv + taps_here[KCONV - 1 - lag] * shifted
    hidden = (jax.nn.silu(conv) * up).astype(jnp.bfloat16)
    down_whole = lax.all_gather(down_proj, FS, axis=1, tiled=True)
    part = hidden
    channel_part = sum_at_owner(
        jnp.dot(part, down_whole, preferred_element_type=jnp.float32).astype(jnp.bfloat16), "tp", 0
    )
    return (middle.astype(jnp.float32) + channel_part).astype(jnp.bfloat16)


def solution(mesh):
    split = Mesh(
        mesh.devices.reshape(mesh.shape["rep"], 2, 4, 4, mesh.shape["tp"]),
        ("rep", "fs_0", "fs_1", "fs_2", "tp"),
    )
    placed = (
        P(REP_FS_TP, None),
        P(),
        P(FS, "tp"),
        P(FS, "tp"),
        P(),
        P(),
        P(),
        P(),
        P("tp", FS),
        P(),
        P(FS, "tp"),
        P(FS, "tp"),
        P(),
        P("tp", FS),
    )
    return jax.shard_map(
        on_device, mesh=split, in_specs=placed, out_specs=P(REP_FS_TP, None), check_vma=False
    )
```

profile of v0, /device:TPU:1, one launch (start us, length us, event | category | flops | bytes accessed | tf_op | source)
XLA Modules:
  0.0 617.4 jit_solution(9370628572742280357)
XLA Ops:
  6.6 6.7 %all-gather = bf16[2048,64]{0,1:T(8,128)(2,1)S(1)} all-gather(bf16[1024,64]{0,1:T(8,128)(2,1)} %param.22), channel_id=2, replica_groups=mesh['rep'=2,'fs_0'=2,'fs_1'=4,'fs_2'=4,'tp'=2] {'fs_0'}, dimensions={0}, use_global_device_ids=true | all-gather | bytes 393216 | tf_op jit(solution)/shard_map/all_gather | solution.py:56
  13.3 0.7 copy.73
  14.1 0.0 all-gather.11.cloned.1.call-start
  14.1 24.9 %all-gather.9.cloned.1.call-done = bf16[8,1024,64]{1,2,0:T(8,128)(2,1)} async-done(((bf16[2,1024,64]{1,2,0:T(8,128)(2,1)}), bf16[8,1024,64]{1,2,0:T(8,128)(2,1)}) %all-gather.9.cloned.1.call-update) | async-done | bytes 1048592 | tf_op jit(solution)/shard_map/all_gather | solution.py:56
  39.1 0.7 pad_maximum_fusion.1
  39.8 0.0 all-gather.13.cloned.1.call-start
  39.9 0.8 pad_maximum_fusion
  40.7 0.5 all-gather.15.cloned.1.call-update
  41.3 1.6 broadcast_in_dim.32
  42.9 6.5 %all-to-all-start = ((bf16[2,256,2048]{2,1,0:T(8,128)(2,1)}), bf16[2,256,2048]{2,1,0:T(8,128)(2,1)S(1)}, u32[]{:S(2)}, u32[]{:S(2)}) async-start(bf16[2,256,2048]{2,1,0:T(8,128)(2,1)} %broadcast_in_dim.32), calls=%async_computation | async-start | bytes 4194304 | tf_op jit(solution)/shard_map/all_to_all | solution.py:25
  49.4 2.5 all-to-all-done
  51.9 0.5 multiply_reduce_fusion.1
  52.4 1.6 dynamic-slice_reduce_fusion.2
  54.0 0.6 fusion.61
  54.6 0.1 broadcast_compare_fusion
  54.7 1.9 fusion.11
  56.5 34.6 %all-gather.11.cloned.1.call-done = bf16[32,1024,64]{1,2,0:T(8,128)(2,1)} async-done(((bf16[8,1024,64]{1,2,0:T(8,128)(2,1)}), bf16[32,1024,64]{1,2,0:T(8,128)(2,1)}) %all-gather.11.cloned.1.call-update) | async-done | bytes 4194320 | tf_op jit(solution)/shard_map/all_gather | solution.py:56
  91.1 4.9 copy.56
  96.0 143.2 %all-gather.7.cloned.1.call-done = bf16[2048,2048]{1,0:T(8,128)(2,1)} async-done(((bf16[64,2048]{1,0:T(8,128)(2,1)}), bf16[2048,2048]{1,0:T(8,128)(2,1)}) %all-gather.7.cloned.1.call-update) | async-done | bytes 8388624 | tf_op jit(solution)/shard_map/all_gather | solution.py:37
  239.2 5.1 fusion.37
  244.3 1.0 fusion.52
  245.3 24.3 %all_to_all.26 = f32[2,1,1024]{2,1,0:T(1,128)S(1)} all-to-all(f32[2,1,1024]{2,1,0:T(1,128)S(1)} %broadcast_in_dim.33), channel_id=1, replica_groups=mesh['rep'=2,'fs_0'=2,'fs_1'=4,'fs_2'=4,'tp'=2] {'tp'}, dimensions={0} | all-to-all | bytes 16384 | tf_op jit(solution)/shard_map/all_to_all | solution.py:25
  269.7 1.0 add_convert_fusion.2
  270.7 2.3 reshape.157
  273.1 2.7 bitcast_add_fusion
  275.8 3.0 copy.60
  278.8 3.5 reshape.158
  282.3 5.4 fusion.34
  287.7 2.7 convolution_convert_fusion
  290.4 5.3 all_to_all.27
  295.8 0.4 convert_reduce_fusion.1
  296.2 0.3 add_convert_fusion.1
  296.6 0.3 broadcast_in_dim.37
  296.8 5.5 all_to_all.28
  302.3 0.5 multiply_reduce_fusion
  302.9 0.2 copy-done.10
  303.0 1.9 fusion.9
  304.9 109.0 %all-gather.13.cloned.1.call-done = bf16[2048,2816]{1,0:T(8,128)(2,1)} async-done(((bf16[64,2816]{1,0:T(8,128)(2,1)}), bf16[2048,2816]{1,0:T(8,128)(2,1)}) %all-gather.13.cloned.1.call-update) | async-done | bytes 11534352 | tf_op jit(solution)/shard_map/all_gather | solution.py:37
  413.9 6.8 %fusion.12 = bf16[512,1408]{1,0:T(8,128)(2,1)S(1)} fusion(bf16[512,2048]{1,0:T(8,128)(2,1)} %fusion.9, bf16[2048,2816]{1,0:T(8,128)(2,1)} %all-gather.13.cloned.1.call-done), kind=kOutput, calls=%fused_computation.27 | convolution fusion | flops 2953510912 | bytes 9306112 | tf_op jit(solution)/shard_map/dot_general | solution.py:144
  420.7 1.7 slice.28
  422.4 1.9 slice.29
  424.3 1.2 copy-done.4
  425.5 4.5 fusion.15
  430.0 144.2 %all-gather.15.cloned.1.call-done = bf16[1408,2048]{0,1:T(8,128)(2,1)} async-done(((bf16[1408,64]{0,1:T(8,128)(2,1)}), bf16[1408,2048]{0,1:T(8,128)(2,1)}) %all-gather.15.cloned.1.call-update) | async-done | bytes 5767184 | tf_op jit(solution)/shard_map/all_gather | solution.py:156
  574.2 9.8 %convolution_convert_fusion.1 = bf16[512,2048]{1,0:T(8,128)(2,1)S(1)} fusion(bf16[1408,2048]{0,1:T(8,128)(2,1)} %all-gather.15.cloned.1.call-done, bf16[512,1408]{1,0:T(8,128)(2,1)} %fusion.15, f32[510,1408]{1,0:T(8,128)} %slice.29, f32[511,1408]{1,0:T(8,128)} %slice.28, f32[1408]{0:T(1024)S(1)} %copy-done.13, f32[1408]{0:T(1024)S(1)} %copy-done.12, ...), kind=kOutput, calls=%fused_computation.29 | convolution fusion | flops 2964652032 | bytes 16516096 | tf_op jit(solution)/shard_map/dot_general | solution.py:159
  584.0 25.1 %all_to_all.29 = bf16[2,256,2048]{2,1,0:T(8,128)(2,1)S(1)} all-to-all(bf16[2,256,2048]{2,1,0:T(8,128)(2,1)S(1)} %bitcast.51), channel_id=1, replica_groups=mesh['rep'=2,'fs_0'=2,'fs_1'=4,'fs_2'=4,'tp'=2] {'tp'}, dimensions={0} | all-to-all | bytes 4194304 | tf_op jit(solution)/shard_map/all_to_all | solution.py:74
  609.1 0.4 convert_reduce_fusion
  609.6 1.3 add_convert_fusion
  (58 shorter events, 0.3 us)
Async XLA Ops:
  6.5 48.0 %copy-start = (f32[32,128]{1,0:T(8,128)S(1)}, f32[32,128]{1,0:T(8,128)}, u32[]{:S(2)}) copy-start(f32[32,128]{1,0:T(8,128)} %param.21) | copy-start | bytes 49156
  6.5 32.5 %copy-start.8 = (bf16[64,1024]{1,0:T(8,128)(2,1)S(1)}, bf16[64,1024]{1,0:T(8,128)(2,1)}, u32[]{:S(2)}) copy-start(bf16[64,1024]{1,0:T(8,128)(2,1)} %param.16) | copy-start | bytes 393220
  6.5 32.5 %copy-start.7 = (bf16[64,1024]{1,0:T(8,128)(2,1)S(1)}, bf16[64,1024]{1,0:T(8,128)(2,1)}, u32[]{:S(2)}) copy-start(bf16[64,1024]{1,0:T(8,128)(2,1)} %param.17) | copy-start | bytes 393220
  6.5 33.3 %copy-start.6 = (bf16[64,1408]{1,0:T(8,128)(2,1)S(1)}, bf16[64,1408]{1,0:T(8,128)(2,1)}, u32[]{:S(2)}) copy-start(bf16[64,1408]{1,0:T(8,128)(2,1)} %param.24) | copy-start | bytes 540676
  6.5 33.3 %copy-start.5 = (bf16[64,1408]{1,0:T(8,128)(2,1)S(1)}, bf16[64,1408]{1,0:T(8,128)(2,1)}, u32[]{:S(2)}) copy-start(bf16[64,1408]{1,0:T(8,128)(2,1)} %param.25) | copy-start | bytes 540676
  6.5 34.7 %copy-start.3 = (bf16[256,2048]{1,0:T(8,128)(2,1)S(1)}, bf16[256,2048]{1,0:T(8,128)(2,1)}, u32[]{:S(2)}) copy-start(bf16[256,2048]{1,0:T(8,128)(2,1)} %param.14) | copy-start | bytes 3145732
  6.6 32.4 %all-gather.9.cloned.1.call-start = ((), (), s32[]{:S(2)}) async-start(), calls=%async_computation.6 | async-start | bytes 1310720 | tf_op jit(solution)/shard_map/all_gather | solution.py:56
  14.1 77.0 %all-gather.11.cloned.1.call-start = ((), (), s32[]{:S(2)}) async-start(), calls=%async_computation.7 | async-start | bytes 5242880 | tf_op jit(solution)/shard_map/all_gather | solution.py:56
  39.0 200.2 %all-gather.7.cloned.1.call-start = ((), (), s32[]{:S(2)}) async-start(), calls=%async_computation.5 | async-start | bytes 8650752 | tf_op jit(solution)/shard_map/all_gather | solution.py:37
  39.8 374.0 %all-gather.13.cloned.1.call-start = ((), (), s32[]{:S(2)}) async-start(), calls=%async_computation.8 | async-start | bytes 11894784 | tf_op jit(solution)/shard_map/all_gather | solution.py:37
  40.7 533.5 %all-gather.15.cloned.1.call-start = ((), (), s32[]{:S(2)}) async-start(), calls=%async_computation.9 | async-start | bytes 5947392 | tf_op jit(solution)/shard_map/all_gather | solution.py:156
  42.9 9.0 %all-to-all-start = ((bf16[2,256,2048]{2,1,0:T(8,128)(2,1)}), bf16[2,256,2048]{2,1,0:T(8,128)(2,1)S(1)}, u32[]{:S(2)}, u32[]{:S(2)}) async-start(bf16[2,256,2048]{2,1,0:T(8,128)(2,1)} %broadcast_in_dim.32), calls=%async_computation | async-start | bytes 4194304 | tf_op jit(solution)/shard_map/all_to_all | solution.py:25
  49.4 5.3 copy-start.9
  96.0 173.8 %dynamic-slice-start = ((f32[2048]{0:T(1024)}, s32[]{:T(128)}), f32[1024]{0:T(1024)S(1)}, s32[]{:S(2)}) async-start(f32[2048]{0:T(1024)} %param.18, s32[]{:T(128)} %select_n.51), calls=%async_computation.10 | async-start | bytes 8704 | tf_op jit(solution)/shard_map/dynamic_slice | solution.py:121
  96.0 173.8 %dynamic-slice-start.1 = ((f32[2048]{0:T(1024)}, s32[]{:T(128)}), f32[1024]{0:T(1024)S(1)}, s32[]{:S(2)}) async-start(f32[2048]{0:T(1024)} %param.19, s32[]{:T(128)} %select_n.51), calls=%async_computation.11 | async-start | bytes 8704 | tf_op jit(solution)/shard_map/dynamic_slice | solution.py:122
  282.3 5.4 copy-start.2
  302.3 0.7 copy-start.10
  413.9 10.4 %slice-start = ((s8[11534336]{0:T(1024)(128)(4,1)}), s8[4194304]{0:T(1024)(128)(4,1)S(1)}, s32[]{:S(2)}) async-start(s8[11534336]{0:T(1024)(128)(4,1)} %bitcast.57), calls=%async_computation.12 | async-start | bytes 8388608
  413.9 10.4 %slice-start.1 = ((s8[11534336]{0:T(1024)(128)(4,1)}), s8[4194304]{0:T(1024)(128)(4,1)S(1)}, s32[]{:S(2)}) async-start(s8[11534336]{0:T(1024)(128)(4,1)} %bitcast.57), calls=%async_computation.13 | async-start | bytes 8388608
  420.7 3.6 slice-start.2
  422.4 3.1 copy-start.4
  425.5 148.7 %copy-start.11 = (f32[1408]{0:T(1024)S(1)}, f32[1408]{0:T(1024)}, u32[]{:S(2)}) copy-start(f32[1408]{0:T(1024)} %get-tuple-element.7) | copy-start | bytes 16900
  425.5 148.7 %copy-start.12 = (f32[1408]{0:T(1024)S(1)}, f32[1408]{0:T(1024)}, u32[]{:S(2)}) copy-start(f32[1408]{0:T(1024)} %get-tuple-element.8) | copy-start | bytes 16900
  425.5 148.7 %copy-start.13 = (f32[1408]{0:T(1024)S(1)}, f32[1408]{0:T(1024)}, u32[]{:S(2)}) copy-start(f32[1408]{0:T(1024)} %get-tuple-element.9) | copy-start | bytes 16900
  425.5 148.7 %copy-start.14 = (pred[512]{0:T(512)(128)(4,1)S(1)}, pred[512]{0:T(512)(128)(4,1)}, u32[]{:S(2)}) copy-start(pred[512]{0:T(512)(128)(4,1)} %get-tuple-element.12) | copy-start | bytes 1540
  425.5 148.7 %copy-start.15 = (pred[512]{0:T(512)(128)(4,1)S(1)}, pred[512]{0:T(512)(128)(4,1)}, u32[]{:S(2)}) copy-start(pred[512]{0:T(512)(128)(4,1)} %get-tuple-element.13) | copy-start | bytes 1540
  609.1 1.8 copy-start.1
Sparse Core Ops, SparseCore 0:
  14.2 24.7 all-gather.8
  40.6 50.3 all-gather.10
  92.7 146.3 all-gather.6
  240.7 173.1 all-gather.12
  415.4 158.7 all-gather.14
where the time goes:
time: 618 us; the launch traced here: 617 us
  waiting for transfers between devices  459 us (74%)
  blocking collectives  67.1 us (11%)
  matrix products  37 us (6%)
  local copies, waits for them, and re-layouts  22.9 us (4%)
  between operations  13.4 us (2%)
  other arithmetic  11.5 us (2%)
  starting transfers between devices  6.7 us (1%)
    all_gather x2, waiting for transfers between devices, side_by_side(): out = lax.all_gather(both, axis, axis=dim, tiled=True)  252 us
    all_gather x1, waiting for transfers between devices, on_device(): down_whole = lax.all_gather(down_proj, FS, axis=1, tiled=True)  144 us
    all_gather x2, waiting for transfers between devices, stacked_from(): pieces = lax.all_gather(pieces, axes[k], axis=0, tiled=True)  59.4 us
    all_to_all x2, blocking collectives, sum_at_owner(): lax.all_to_all(pieces, axis, split_axis=0, concat_axis=0, tiled=True)  30.5 us
    all_to_all x2, blocking collectives, copy_for_each(): lax.all_to_all(jnp.broadcast_to(value[None], (devices, *value.shape)), ax...  29.9 us
  transfers between devices with their start and end apart: 6, of which 6 were waited for; matrix products, arithmetic and copies ran while one was open for 9% of the time, Pallas kernels for 0%

commit v1 on v0

--- a/solution.py
+++ b/solution.py
@@ -153,7 +153,9 @@
         shifted = jnp.where((offset >= lag)[:, None], shifted, 0.0)
         conv = conv + taps_here[KCONV - 1 - lag] * shifted
     hidden = (jax.nn.silu(conv) * up).astype(jnp.bfloat16)
-    down_whole = lax.all_gather(down_proj, FS, axis=1, tiled=True)
+    down_whole = jnp.concatenate(
+        lax.all_to_all(jnp.stack([down_proj] * lax.axis_size(FS)), FS, 0, 0), axis=1
+    )
     part = hidden
     channel_part = sum_at_owner(
         jnp.dot(part, down_whole, preferred_element_type=jnp.float32).astype(jnp.bfloat16), "tp", 0

time: 618 us -> 537 us (0.87)
  waiting for transfers between devices: 459 us -> 374 us
  starting transfers between devices: 6.7 us -> 14 us
    all_gather x1 -> x0, waiting for transfers between devices: 144 us -> none  [on_device(): down_whole = lax.all_gather(down_proj, FS, axis=1, tiled=True)]
    all_gather x2, waiting for transfers between devices: 252 us -> 309 us  [side_by_side(): out = lax.all_gather(both, axis, axis=dim, tiled=True)]
    all_to_all x0 -> x1, starting transfers between devices: none -> 7.37 us  [on_device(): lax.all_to_all(jnp.stack([down_proj] * lax.axis_size(FS)), FS, 0, 0)]
  transfers between devices with their start and end apart: 6 -> 6, of which waited for: 6 -> 5; matrix products, arithmetic and copies ran while one was open for 9% -> 11% of each run, Pallas kernels for 0% -> 0%
where the time goes in v1:
time: 537 us
  waiting for transfers between devices  374 us (70%)
  blocking collectives  62.1 us (12%)
  matrix products  37 us (7%)
  local copies, waits for them, and re-layouts  25.4 us (5%)
  starting transfers between devices  14 us (3%)
  between operations  13.4 us (2%)
  other arithmetic  11 us (2%)
    all_gather x2, waiting for transfers between devices, side_by_side(): out = lax.all_gather(both, axis, axis=dim, tiled=True)  309 us
    all_gather x2, waiting for transfers between devices, stacked_from(): pieces = lax.all_gather(pieces, axes[k], axis=0, tiled=True)  62 us
    all_to_all x2, blocking collectives, copy_for_each(): lax.all_to_all(jnp.broadcast_to(value[None], (devices, *value.shape)), ax...  29.9 us
    all_to_all x2, blocking collectives, sum_at_owner(): lax.all_to_all(pieces, axis, split_axis=0, concat_axis=0, tiled=True)  25.5 us
  transfers between devices with their start and end apart: 6, of which 5 were waited for; matrix products, arithmetic and copies ran while one was open for 11% of the time, Pallas kernels for 0%

profile of v1, /device:TPU:1, one launch (start us, length us, event | category | flops | bytes accessed | tf_op | source)
XLA Modules:
  0.0 536.7 jit_solution(10030381703385342435)
XLA Ops:
  6.6 0.0 all-gather.8.cloned.1.call-start
  6.6 6.7 %all-gather = bf16[2048,64]{0,1:T(8,128)(2,1)S(1)} all-gather(bf16[1024,64]{0,1:T(8,128)(2,1)} %param.22), channel_id=2, replica_groups=mesh['rep'=2,'fs_0'=2,'fs_1'=4,'fs_2'=4,'tp'=2] {'fs_0'}, dimensions={0}, use_global_device_ids=true | all-gather | bytes 393216 | tf_op jit(solution)/shard_map/all_gather | solution.py:56
  13.3 0.7 copy.74
  14.1 0.0 all-gather.10.cloned.1.call-start
  14.1 24.9 %all-gather.8.cloned.1.call-done = bf16[8,1024,64]{1,2,0:T(8,128)(2,1)} async-done(((bf16[2,1024,64]{1,2,0:T(8,128)(2,1)}), bf16[8,1024,64]{1,2,0:T(8,128)(2,1)}) %all-gather.8.cloned.1.call-update) | async-done | bytes 1048592 | tf_op jit(solution)/shard_map/all_gather | solution.py:56
  39.0 0.0 all-gather.6.cloned.1.call-start
  39.1 0.7 pad_maximum_fusion.1
  39.8 0.0 all-gather.12.cloned.1.call-start
  39.9 0.8 pad_maximum_fusion
  40.7 1.6 broadcast_in_dim.32
  42.3 6.5 %all-to-all-start = ((bf16[2,256,2048]{2,1,0:T(8,128)(2,1)}), bf16[2,256,2048]{2,1,0:T(8,128)(2,1)S(1)}, u32[]{:S(2)}, u32[]{:S(2)}) async-start(bf16[2,256,2048]{2,1,0:T(8,128)(2,1)} %broadcast_in_dim.32), calls=%async_computation | async-start | bytes 4194304 | tf_op jit(solution)/shard_map/all_to_all | solution.py:25
  48.8 2.5 all-to-all-done
  51.3 0.5 multiply_reduce_fusion.1
  51.9 0.1 broadcast_compare_fusion
  52.0 2.0 fusion.11
  54.0 37.1 %all-gather.10.cloned.1.call-done = bf16[32,1024,64]{1,2,0:T(8,128)(2,1)} async-done(((bf16[8,1024,64]{1,2,0:T(8,128)(2,1)}), bf16[32,1024,64]{1,2,0:T(8,128)(2,1)}) %all-gather.10.cloned.1.call-update) | async-done | bytes 4194320 | tf_op jit(solution)/shard_map/all_gather | solution.py:56
  91.1 5.0 copy.57
  96.1 143.1 %all-gather.6.cloned.1.call-done = bf16[2048,2048]{1,0:T(8,128)(2,1)} async-done(((bf16[64,2048]{1,0:T(8,128)(2,1)}), bf16[2048,2048]{1,0:T(8,128)(2,1)}) %all-gather.6.cloned.1.call-update) | async-done | bytes 8388624 | tf_op jit(solution)/shard_map/all_gather | solution.py:37
  239.2 5.2 fusion.37
  244.3 1.0 fusion.52
  245.3 24.3 %all_to_all.31 = f32[2,1,1024]{2,1,0:T(1,128)S(1)} all-to-all(f32[2,1,1024]{2,1,0:T(1,128)S(1)} %broadcast_in_dim.33), channel_id=1, replica_groups=mesh['rep'=2,'fs_0'=2,'fs_1'=4,'fs_2'=4,'tp'=2] {'tp'}, dimensions={0} | all-to-all | bytes 16384 | tf_op jit(solution)/shard_map/all_to_all | solution.py:25
  269.7 1.0 add_convert_fusion.2
  270.8 2.3 reshape.167
  273.1 2.7 bitcast_add_fusion
  275.8 3.0 copy.61
  278.8 3.5 reshape.168
  282.3 5.4 fusion.34
  287.7 2.7 convolution_convert_fusion
  290.4 5.4 all_to_all.32
  295.7 0.4 convert_reduce_fusion.1
  296.2 0.3 add_convert_fusion.1
  296.5 0.2 broadcast_in_dim.37
  296.8 5.5 %all_to_all.33 = bf16[2,256,2048]{2,1,0:T(8,128)(2,1)S(1)} all-to-all(bf16[2,256,2048]{2,1,0:T(8,128)(2,1)S(1)} %broadcast_in_dim.37), channel_id=1, replica_groups=mesh['rep'=2,'fs_0'=2,'fs_1'=4,'fs_2'=4,'tp'=2] {'tp'}, dimensions={0} | all-to-all | bytes 4194304 | tf_op jit(solution)/shard_map/all_to_all | solution.py:25
  302.3 3.2 stack.2
  305.5 7.4 %all-to-all-start.4 = ((bf16[32,1408,64]{1,2,0:T(8,128)(2,1)}), bf16[32,1408,64]{1,2,0:T(8,128)(2,1)}, u32[]{:S(2)}, u32[]{:S(2)}) async-start(bf16[32,1408,64]{1,2,0:T(8,128)(2,1)} %stack.2), calls=%async_computation.4 | async-start | bytes 11534336 | tf_op jit(solution)/shard_map/all_to_all | solution.py:157
  312.9 1.0 dynamic-slice_reduce_fusion.2
  313.9 0.5 multiply_reduce_fusion
  314.4 1.9 fusion.9
  316.3 166.0 %all-gather.12.cloned.1.call-done = bf16[2048,2816]{1,0:T(8,128)(2,1)} async-done(((bf16[64,2816]{1,0:T(8,128)(2,1)}), bf16[2048,2816]{1,0:T(8,128)(2,1)}) %all-gather.12.cloned.1.call-update) | async-done | bytes 11534352 | tf_op jit(solution)/shard_map/all_gather | solution.py:37
  482.3 6.8 %fusion.12 = bf16[512,1408]{1,0:T(8,128)(2,1)S(1)} fusion(bf16[512,2048]{1,0:T(8,128)(2,1)} %fusion.9, bf16[2048,2816]{1,0:T(8,128)(2,1)} %all-gather.12.cloned.1.call-done), kind=kOutput, calls=%fused_computation.27 | convolution fusion | flops 2953510912 | bytes 9306112 | tf_op jit(solution)/shard_map/dot_general | solution.py:144
  489.1 1.7 slice.28
  490.9 1.8 slice.29
  492.7 1.2 copy-done.4
  493.9 4.5 fusion.15
  498.4 9.8 %convolution_convert_fusion.1 = bf16[512,2048]{1,0:T(8,128)(2,1)S(1)} fusion(bf16[1408,2048]{0,1:T(8,128)(2,1)} %bitcast.13, bf16[512,1408]{1,0:T(8,128)(2,1)} %fusion.15, f32[510,1408]{1,0:T(8,128)} %slice.29, f32[511,1408]{1,0:T(8,128)} %slice.28, f32[1408]{0:T(1024)S(1)} %get-tuple-element.9, f32[1408]{0:T(1024)S(1)} %get-tuple-element.8, ...), kind=kOutput, calls=%fused_computation.29 | convolution fusion | flops 2964652032 | bytes 16516096 | tf_op jit(solution)/shard_map/dot_general | solution.py:161
  508.2 20.2 %all_to_all.34 = bf16[2,256,2048]{2,1,0:T(8,128)(2,1)S(1)} all-to-all(bf16[2,256,2048]{2,1,0:T(8,128)(2,1)S(1)} %bitcast.54), channel_id=1, replica_groups=mesh['rep'=2,'fs_0'=2,'fs_1'=4,'fs_2'=4,'tp'=2] {'tp'}, dimensions={0} | all-to-all | bytes 4194304 | tf_op jit(solution)/shard_map/all_to_all | solution.py:74
  528.4 0.4 convert_reduce_fusion
  528.8 1.3 add_convert_fusion
  (50 shorter events, 0.2 us)
Async XLA Ops:
  6.5 45.3 %copy-start = (f32[32,128]{1,0:T(8,128)S(1)}, f32[32,128]{1,0:T(8,128)}, u32[]{:S(2)}) copy-start(f32[32,128]{1,0:T(8,128)} %param.21) | copy-start | bytes 49156
  6.5 32.5 %copy-start.9 = (bf16[64,1024]{1,0:T(8,128)(2,1)S(1)}, bf16[64,1024]{1,0:T(8,128)(2,1)}, u32[]{:S(2)}) copy-start(bf16[64,1024]{1,0:T(8,128)(2,1)} %param.16) | copy-start | bytes 393220
  6.5 32.5 %copy-start.8 = (bf16[64,1024]{1,0:T(8,128)(2,1)S(1)}, bf16[64,1024]{1,0:T(8,128)(2,1)}, u32[]{:S(2)}) copy-start(bf16[64,1024]{1,0:T(8,128)(2,1)} %param.17) | copy-start | bytes 393220
  6.5 33.3 %copy-start.7 = (bf16[64,1408]{1,0:T(8,128)(2,1)S(1)}, bf16[64,1408]{1,0:T(8,128)(2,1)}, u32[]{:S(2)}) copy-start(bf16[64,1408]{1,0:T(8,128)(2,1)} %param.24) | copy-start | bytes 540676
  6.5 33.3 %copy-start.6 = (bf16[64,1408]{1,0:T(8,128)(2,1)S(1)}, bf16[64,1408]{1,0:T(8,128)(2,1)}, u32[]{:S(2)}) copy-start(bf16[64,1408]{1,0:T(8,128)(2,1)} %param.25) | copy-start | bytes 540676
  6.5 34.1 %copy-start.3 = (bf16[256,2048]{1,0:T(8,128)(2,1)S(1)}, bf16[256,2048]{1,0:T(8,128)(2,1)}, u32[]{:S(2)}) copy-start(bf16[256,2048]{1,0:T(8,128)(2,1)} %param.14) | copy-start | bytes 3145732
  6.6 32.4 %all-gather.8.cloned.1.call-start = ((), (), s32[]{:S(2)}) async-start(), calls=%async_computation.7 | async-start | bytes 1310720 | tf_op jit(solution)/shard_map/all_gather | solution.py:56
  14.1 77.0 %all-gather.10.cloned.1.call-start = ((), (), s32[]{:S(2)}) async-start(), calls=%async_computation.8 | async-start | bytes 5242880 | tf_op jit(solution)/shard_map/all_gather | solution.py:56
  39.0 200.2 %all-gather.6.cloned.1.call-start = ((), (), s32[]{:S(2)}) async-start(), calls=%async_computation.6 | async-start | bytes 8650752 | tf_op jit(solution)/shard_map/all_gather | solution.py:37
  39.8 442.5 %all-gather.12.cloned.1.call-start = ((), (), s32[]{:S(2)}) async-start(), calls=%async_computation.9 | async-start | bytes 11894784 | tf_op jit(solution)/shard_map/all_gather | solution.py:37
  42.3 9.0 %all-to-all-start = ((bf16[2,256,2048]{2,1,0:T(8,128)(2,1)}), bf16[2,256,2048]{2,1,0:T(8,128)(2,1)S(1)}, u32[]{:S(2)}, u32[]{:S(2)}) async-start(bf16[2,256,2048]{2,1,0:T(8,128)(2,1)} %broadcast_in_dim.32), calls=%async_computation | async-start | bytes 4194304 | tf_op jit(solution)/shard_map/all_to_all | solution.py:25
  48.8 3.1 copy-start.10
  96.1 173.7 %dynamic-slice-start = ((f32[2048]{0:T(1024)}, s32[]{:T(128)}), f32[1024]{0:T(1024)S(1)}, s32[]{:S(2)}) async-start(f32[2048]{0:T(1024)} %param.18, s32[]{:T(128)} %select_n.51), calls=%async_computation.10 | async-start | bytes 8704 | tf_op jit(solution)/shard_map/dynamic_slice | solution.py:121
  96.1 173.7 %dynamic-slice-start.1 = ((f32[2048]{0:T(1024)}, s32[]{:T(128)}), f32[1024]{0:T(1024)S(1)}, s32[]{:S(2)}) async-start(f32[2048]{0:T(1024)} %param.19, s32[]{:T(128)} %select_n.51), calls=%async_computation.11 | async-start | bytes 8704 | tf_op jit(solution)/shard_map/dynamic_slice | solution.py:122
  282.3 5.4 %copy-start.2 = (bf16[2,4,4,1024,64]{3,4,2,1,0:T(8,128)(2,1)S(1)}, bf16[2,4,4,1024,64]{3,4,2,1,0:T(8,128)(2,1)}, u32[]{:S(2)}) copy-start(bf16[2,4,4,1024,64]{3,4,2,1,0:T(8,128)(2,1)} %copy.57) | copy-start | bytes 12582916
  296.8 5.6 %copy-start.5 = (bf16[1408,64]{0,1:T(8,128)(2,1)S(1)}, bf16[1408,64]{0,1:T(8,128)(2,1)}, u32[]{:S(2)}) copy-start(bf16[1408,64]{0,1:T(8,128)(2,1)} %param.27) | copy-start | bytes 540676
  305.5 192.9 %all-to-all-start.4 = ((bf16[32,1408,64]{1,2,0:T(8,128)(2,1)}), bf16[32,1408,64]{1,2,0:T(8,128)(2,1)}, u32[]{:S(2)}, u32[]{:S(2)}) async-start(bf16[32,1408,64]{1,2,0:T(8,128)(2,1)} %stack.2), calls=%async_computation.4 | async-start | bytes 11534336 | tf_op jit(solution)/shard_map/all_to_all | solution.py:157
  312.9 1.5 copy-start.11
  482.3 10.4 %slice-start = ((s8[11534336]{0:T(1024)(128)(4,1)}), s8[4194304]{0:T(1024)(128)(4,1)S(1)}, s32[]{:S(2)}) async-start(s8[11534336]{0:T(1024)(128)(4,1)} %bitcast.60), calls=%async_computation.12 | async-start | bytes 8388608
  482.3 10.4 %slice-start.1 = ((s8[11534336]{0:T(1024)(128)(4,1)}), s8[4194304]{0:T(1024)(128)(4,1)S(1)}, s32[]{:S(2)}) async-start(s8[11534336]{0:T(1024)(128)(4,1)} %bitcast.60), calls=%async_computation.13 | async-start | bytes 8388608
  489.1 3.6 slice-start.2
  490.9 3.0 copy-start.4
  528.4 1.8 copy-start.1
Sparse Core Ops, SparseCore 0:
  14.2 24.7 all-gather.7
  40.6 50.3 all-gather.9
  92.7 146.3 all-gather.5
  240.7 241.5 all-gather.11
